TPU v7x, 32 devices: a whole 2x2x4 slice. The times are simulated.
32 devices in a mesh: ep: 8 (over z, x), tp: 4 (over y, core).
Axes of the slice: x: 2, y: 2, z: 4, core: 2. Of those that a mesh axis runs over, the one named last changes fastest.
Arguments:
- queries: bfloat16 [2048, 8, 128], P('ep', 'tp'), may hold values from -256 to 256
- keys: bfloat16 [2048, 4, 128], P('ep', 'tp'), may hold values from -8 to 8
- values: bfloat16 [2048, 4, 128], P('ep', 'tp'), may hold values from -6 to 6
- attn_lambda: float32 [8], P('tp'), may hold values from 0.3 to 0.8
- head_gain: float32 [128], replicated, may hold values from 0.1 to 1.9
- w_out: bfloat16 [1024, 2048], replicated, may hold values from -0.1875 to 0.1875
- moe_rows: bfloat16 [4096, 2048], P('ep'), may hold values from -6 to 6
- moe_gain: float32 [2048], replicated, may hold values from 0.1 to 1.9
- routes: int32 [4096, 2], P('ep'), may hold values from 0 to 7, all different within a row; in each aligned block of 128 rows (0 to 127, 128 to 255, ...) at most 64 rows name the same one
- route_weights: float32 [4096, 2], P('ep'), may hold values from 0.1 to 1
- w_gate: bfloat16 [8, 2048, 1024], P('ep', None, 'tp'), may hold values from -0.125 to 0.125
- w_up: bfloat16 [8, 2048, 1024], P('ep', None, 'tp'), may hold values from -0.125 to 0.125
- w_down: bfloat16 [8, 1024, 2048], P('ep', 'tp'), may hold values from -0.1875 to 0.1875
Outputs:
- mixer_out: bfloat16 [2048, 2048], P(('ep', 'tp'))
- moe_out: bfloat16 [4096, 2048], P(('ep', 'tp'))
Inputs may be any that keep to these rules, and one draw needn't show every extreme that they name: `routes`: each row names 2 different experts. In each aligned block of 128 rows (the rows of moe_out that one device holds) no expert is named by more than 64 rows, a bound that some block reaches.
All inputs are finite; a program needn't handle non-finite values.
Results may differ from a plain program's by a relative error of at most 0.011.
Values may be sent and summed in bfloat16 or wider, within the bound.
A program may use at most 128 MiB of HBM per device.

v0:
```python
import jax
import jax.numpy as jnp
from jax import lax
from jax.sharding import PartitionSpec as P

EPSILON = 1e-06
MASKED = -1e30


def rms_scaled(values_f, gain):
    mean_sq = jnp.mean(values_f * values_f, axis=-1, keepdims=True)
    return values_f * lax.rsqrt(mean_sq + EPSILON) * gain


def slot_numbers(block_routes, experts):
    flat_ids = block_routes.reshape(-1)
    matches = (flat_ids[:, None] == lax.iota(jnp.int32, experts)[None, :]).astype(jnp.int32)
    earlier = jnp.cumsum(matches, axis=0) - matches
    return jnp.sum(earlier * matches, axis=1).reshape(block_routes.shape)


def fill_slots(block_rows, block_routes, experts, capacity):
    slot_ids = slot_numbers(block_routes, experts)
    model_width = block_rows.shape[1]
    copies = jnp.broadcast_to(block_rows[:, None, :], block_routes.shape + (model_width,))
    blank_slots = jnp.zeros((experts, capacity, model_width), block_rows.dtype)
    return (blank_slots.at[block_routes, slot_ids].set(copies), slot_ids)


def local(
    queries,
    keys,
    values,
    attn_lambda,
    head_gain,
    w_out,
    moe_rows,
    moe_gain,
    routes,
    route_weights,
    w_gate,
    w_up,
    w_down,
):
    positions = queries.shape[0]
    q_heads = queries.shape[1]
    kv_heads = keys.shape[1]
    head_dim = queries.shape[2] // 2
    value_dim = values.shape[2]
    per_key = q_heads // kv_heads
    first_pos = lax.axis_index("ep") * positions
    query_pos = first_pos + lax.iota(jnp.int32, positions)
    last_pos = first_pos + positions - 1
    query_view = queries.reshape(positions, kv_heads, per_key, 2, head_dim)
    inv_scale = head_dim ** (-0.5)
    start_max = jnp.full((positions, kv_heads, per_key, 2), MASKED, jnp.float32)
    start_total = jnp.zeros((positions, kv_heads, per_key, 2), jnp.float32)
    start_acc = jnp.zeros((positions, kv_heads, per_key, 2, value_dim), jnp.float32)
    carry = (start_max, start_total, start_acc)
    key_piece = lax.all_gather(keys, "ep", axis=0, tiled=True)
    value_piece = lax.all_gather(values, "ep", axis=0, tiled=True)
    shard_count = key_piece.shape[0] // positions
    together = 1
    for candidate in (2, 3, 4):
        if shard_count % candidate == 0:
            together = candidate
    block_len = together * positions
    blocks = shard_count // together
    key_blocks = key_piece.reshape(blocks, block_len, kv_heads, 2, head_dim)
    value_blocks = value_piece.reshape(blocks, block_len, kv_heads, value_dim)
    block_starts = block_len * lax.iota(jnp.int32, blocks)

    def visit(running, inputs):
        key_blk, value_blk, block_start = inputs

        def update(current):
            run_max, run_total, run_acc = current
            key_pos = block_start + lax.iota(jnp.int32, block_len)
            scores = (
                jnp.einsum(
                    "qkgmd,pkmd->qkgmp", query_view, key_blk, preferred_element_type=jnp.float32
                )
                * inv_scale
            )
            allowed = key_pos[None, :] <= query_pos[:, None]
            scores = jnp.where(allowed[:, None, None, None, :], scores, MASKED)
            new_max = jnp.maximum(run_max, jnp.max(scores, axis=-1))
            shrink = jnp.exp(run_max - new_max)
            weights = jnp.exp(scores - new_max[..., None])
            run_total = run_total * shrink + jnp.sum(weights, axis=-1)
            run_acc = run_acc * shrink[..., None] + jnp.einsum(
                "qkgmp,pkv->qkgmv",
                weights.astype(jnp.bfloat16),
                value_blk,
                preferred_element_type=jnp.float32,
            )
            return (new_max, run_total, run_acc)

        def keep(current):
            return current

        return (lax.cond(block_start <= last_pos, update, keep, running), None)

    carry, unused = lax.scan(visit, carry, (key_blocks, value_blocks, block_starts))
    run_max, run_total, run_acc = carry
    ratios = run_acc / run_total[..., None]
    lambda_view = attn_lambda.reshape(1, kv_heads, per_key, 1)
    head_out = ratios[:, :, :, 0] - lambda_view * ratios[:, :, :, 1]
    attn_rows = (
        rms_scaled(head_out, head_gain).astype(jnp.bfloat16).reshape(positions, q_heads * value_dim)
    )
    tp_count = lax.axis_size("tp")
    tp_id = lax.axis_index("tp")
    exchanged = lax.all_to_all(
        attn_rows.reshape(positions, q_heads, value_dim),
        "tp",
        split_axis=0,
        concat_axis=1,
        tiled=True,
    )
    mixer_out = jnp.dot(
        exchanged.reshape(positions // tp_count, tp_count * q_heads * value_dim),
        w_out,
        preferred_element_type=jnp.float32,
    ).astype(jnp.bfloat16)
    experts = lax.axis_size("ep")
    dev_rows = moe_rows.shape[0] // tp_count
    top_count = routes.shape[1]
    capacity = max(2, 2 * dev_rows * top_count // experts)
    model_width = moe_rows.shape[1]
    hidden_units = w_gate.shape[2]
    own_routes = lax.dynamic_slice_in_dim(routes, tp_id * dev_rows, dev_rows, 0)
    own_weights = lax.dynamic_slice_in_dim(route_weights, tp_id * dev_rows, dev_rows, 0)
    own_rows = rms_scaled(
        lax.dynamic_slice_in_dim(moe_rows, tp_id * dev_rows, dev_rows, 0).astype(jnp.float32),
        moe_gain,
    ).astype(jnp.bfloat16)
    outgoing, own_slots = fill_slots(own_rows, own_routes, experts, capacity)
    arrived = lax.all_to_all(outgoing, "ep", split_axis=0, concat_axis=0, tiled=True)
    slot_rows = lax.all_gather(arrived[None], "tp", axis=0, tiled=True)
    flat_rows = slot_rows.reshape(-1, model_width)
    gate_out = jnp.dot(flat_rows, w_gate[0], preferred_element_type=jnp.float32)
    up_out = jnp.dot(flat_rows, w_up[0], preferred_element_type=jnp.float32)
    hidden = (
        (jax.nn.silu(gate_out) * up_out)
        .astype(jnp.bfloat16)
        .reshape(slot_rows.shape[:-1] + (hidden_units,))
    )
    flat_terms = hidden.reshape(-1, hidden_units)
    summed = lax.psum_scatter(
        jnp.dot(flat_terms, w_down[0], preferred_element_type=jnp.float32)
        .reshape(hidden.shape[:-1] + (model_width,))
        .astype(jnp.bfloat16),
        "tp",
        scatter_dimension=0,
        tiled=True,
    )
    returned = lax.all_to_all(summed, "ep", split_axis=1, concat_axis=1, tiled=True)[0]
    picked = returned[own_routes, own_slots]
    moe_out = jnp.sum(own_weights[..., None] * picked.astype(jnp.float32), axis=1).astype(
        jnp.bfloat16
    )
    return (mixer_out, moe_out)


def solution(mesh):
    return jax.shard_map(
        local,
        mesh=mesh,
        in_specs=(
            P("ep", "tp", None),
            P("ep", "tp", None),
            P("ep", "tp", None),
            P("tp"),
            P(),
            P(),
            P("ep", None),
            P(),
            P("ep", None),
            P("ep", None),
            P("ep", None, "tp"),
            P("ep", None, "tp"),
            P("ep", "tp", None),
        ),
        out_specs=(P(("ep", "tp"), None), P(("ep", "tp"), None)),
        check_vma=False,
    )
```

profile of v0, /device:TPU:0, one launch (start us, length us, event | category | flops | bytes accessed | tf_op | source)
XLA Modules:
  0.0 330.0 jit_solution(4695768976303798606)
XLA Ops:
  7.2 0.0 copy-start
  7.2 0.0 all-gather.3.cloned.1.call-start
  7.2 0.8 constant_dynamic-slice_fusion
  8.0 0.1 copy.83
  8.1 0.1 eq.29
  8.2 0.1 eq.25
  8.4 0.6 reduce-window.6
  9.0 0.2 slice_reduce_fusion
  9.2 0.1 fusion.43
  9.3 0.1 reshape.223
  9.5 0.1 reshape.231
  9.7 1.2 fusion.24
  10.9 1.3 fusion.26
  12.2 0.6 broadcast_in_dim.60
  12.8 1.2 reshape.233
  14.1 0.2 broadcast_in_dim.58
  14.3 33.4 %scatter_fusion = bf16[8,64,2048]{2,1,0:T(8,128)(2,1)S(1)} fusion(bf16[8,64,2048]{2,1,0:T(8,128)(2,1)S(1)} %broadcast_in_dim.58, s32[256]{0:T(256)S(1)} %reshape.231, bf16[256,2048]{1,0:T(8,128)(2,1)} %reshape.233), kind=kCustom, calls=%fused_computation.1 | custom fusion | bytes 3147776 | tf_op jit(solution)/shard_map/scatter | solution.py:27
  47.7 55.4 %all_to_all.25 = bf16[8,64,2048]{2,1,0:T(8,128)(2,1)} all-to-all(bf16[8,64,2048]{2,1,0:T(8,128)(2,1)S(1)} %scatter_fusion), channel_id=1, replica_groups=mesh['ep'=8,'tp'=4] {'ep'}, dimensions={0} | all-to-all | bytes 4194304 | tf_op jit(solution)/shard_map/all_to_all | solution.py:139
  103.1 0.0 all-gather.3.cloned.1.call-update
  103.1 0.0 reduce-scatter.2.cloned.1.call-start
  103.2 57.4 %all-gather.3.cloned.1.call-done = bf16[32,64,2048]{2,1,0:T(8,128)(2,1)} async-done(((bf16[8,64,2048]{2,1,0:T(8,128)(2,1)}), bf16[32,64,2048]{2,1,0:T(8,128)(2,1)}) %all-gather.3.cloned.1.call-update) | async-done | bytes 8388624 | tf_op jit(solution)/shard_map/all_gather | solution.py:140
  160.6 5.9 %fusion.29 = f32[2048,256]{1,0:T(8,128)S(1)} fusion(bf16[2048,2048]{1,0:T(8,128)(2,1)} %bitcast.134, bf16[1,2048,256]{2,1,0:T(8,128)(2,1)S(1)} %copy-done.7), kind=kOutput, calls=%fused_computation.40 | convolution fusion | flops 2147483648 | bytes 11534336 | tf_op jit(solution)/shard_map/dot_general | solution.py:142
  166.5 0.0 copy-done.6
  166.5 0.1 copy-done.8
  166.6 2.6 fusion.23
  169.2 0.0 copy-done
  169.2 5.6 %convolution_convert_fusion = bf16[4,8,64,2048]{3,2,1,0:T(8,128)(2,1)} fusion(bf16[4,8,64,256]{3,2,1,0:T(8,128)(2,1)S(1)} %bitcast.130, bf16[1,256,2048]{2,1,0:T(8,128)(2,1)S(1)} %copy-done), kind=kOutput, calls=%fused_computation.28 | convolution fusion | flops 2151677952 | bytes 10485760 | tf_op jit(solution)/shard_map/dot_general | solution.py:151
  174.8 0.0 reduce-scatter.2.cloned.1.call-update
  174.8 0.0 copy-start.3
  174.8 0.8 copy-done.2
  175.6 31.4 %all_gather.9 = bf16[2048,1,128]{2,0,1:T(8,128)(2,1)S(1)} all-gather(bf16[256,1,128]{2,0,1:T(8,128)(2,1)S(1)} %copy-done.2), channel_id=1, replica_groups=mesh['ep'=8,'tp'=4] {'ep'}, dimensions={0}, use_global_device_ids=true | all-gather | bytes 589824 | tf_op jit(solution)/shard_map/all_gather | solution.py:60
  207.1 0.4 reshape.243
  207.5 0.7 copy.64
  208.3 31.4 %all_gather.10 = bf16[2048,1,128]{2,0,1:T(8,128)(2,1)S(1)} all-gather(bf16[256,1,128]{2,0,1:T(8,128)(2,1)S(1)} %copy-done.3), channel_id=1, replica_groups=mesh['ep'=8,'tp'=4] {'ep'}, dimensions={0}, use_global_device_ids=true | all-gather | bytes 589824 | tf_op jit(solution)/shard_map/all_gather | solution.py:61
  239.7 0.2 copy.66
  239.9 0.1 copy.63
  240.1 5.6 %while.15 = (s32[]{:T(128)}, f32[256,1,2,2]{0,2,3,1:T(2,128)S(1)}, f32[256,1,2,2]{0,2,3,1:T(2,128)S(1)}, f32[256,1,2,2,128]{0,4,3,2,1:T(8,128)S(1)}, s32[2]{0:T(...) while((s32[]{:T(128)}, f32[256,1,2,2]{0,2,3,1:T(2,128)S(1)}, ...), condition=%wide.region_5.6_spmd.clone, body=%wide.region_0.5_spmd.clone.sunk | while | flops 411570432 | bytes 15155487 | solution.py:104
  240.2 0.6 dynamic_slice.50
  241.3 3.3 conditional.3
  241.3 0.6 iota_add_fusion
  241.9 0.2 broadcast_compare_fusion
  242.1 0.9 fusion.4
  243.0 1.0 fusion.5
  244.0 0.5 fusion.11
  244.6 0.6 dynamic_slice.50
  245.7 0.0 copy-start.4
  245.7 0.0 copy-start.5
  245.8 0.2 copy.68
  246.0 0.1 copy.67
  246.1 0.7 broadcast_divide_fusion
  246.9 0.4 fusion.33
  247.4 0.4 fusion.37
  247.8 7.0 %all_to_all.26 = bf16[256,2,128]{2,1,0:T(2,128)(2,1)S(1)} all-to-all(bf16[256,2,128]{2,1,0:T(2,128)(2,1)S(1)} %fusion.37), channel_id=1, replica_groups=mesh['ep'=8,'tp'=4] {'tp'}, dimensions={0} | all-to-all | bytes 262144 | tf_op jit(solution)/shard_map/all_to_all | solution.py:114
  254.8 8.9 %all-to-all-start.2 = ((bf16[1,8,64,2048]{3,2,0,1:T(8,128)(2,1)}), bf16[1,8,64,2048]{3,2,0,1:T(8,128)(2,1)S(1)}, u32[]{:S(2)}, u32[]{:S(2)}) async-start(bf16[1,8,64,2048]{3,2,0,1:T(8,128)(2,1)} %bitcast.127), calls=%async_computation.3 | async-start | bytes 4194304 | tf_op jit(solution)/shard_map/all_to_all | solution.py:158
  263.7 0.1 reshape.225
  263.9 0.7 constant_dynamic-slice_fusion.1
  264.5 0.1 copy.73
  264.7 0.1 copy.72
  264.8 0.1 reshape.221
  264.9 3.7 %convolution_convert_fusion.1 = bf16[64,2048]{1,0:T(8,128)(2,1)} fusion(bf16[64,1024]{1,0:T(8,128)(2,1)S(1)} %reshape.221, bf16[1024,2048]{1,0:T(8,128)(2,1)} %param.22), kind=kOutput, calls=%fused_computation.31 | convolution fusion | flops 268566528 | bytes 4587520 | tf_op jit(solution)/shard_map/dot_general | solution.py:121
  268.6 42.9 %all-to-all-done.2 = bf16[1,8,64,2048]{3,2,0,1:T(8,128)(2,1)S(1)} async-done(((bf16[1,8,64,2048]{3,2,0,1:T(8,128)(2,1)}), bf16[1,8,64,2048]{3,2,0,1:T(8,128)(2,1)S(1)}, u32[]{:S(2)}, u32[]{:S(2)}) %all-to-all-start.2) | async-done | bytes 2097184 | tf_op jit(solution)/shard_map/all_to_all | solution.py:158
  311.6 5.3 %gather_fusion = bf16[256,2048]{1,0:T(8,128)(2,1)} fusion(bf16[8,64,2048]{2,1,0:T(8,128)(2,1)S(1)} %bitcast.126, s32[256]{0:T(256)S(1)} %reshape.225), kind=kCustom, calls=%fused_computation | custom fusion | bytes 2099200 | tf_op jit(solution)/shard_map/gather | solution.py:159
  316.9 2.4 reshape.239
  319.3 3.9 %multiply_reduce_fusion = bf16[128,2048]{1,0:T(8,128)(2,1)} fusion(f32[128,2,2048]{2,1,0:T(2,128)S(1)} %reshape.239, f32[128,2]{1,0:T(8,128)S(1)} %copy.73), kind=kLoop, calls=%fused_computation.32 | loop fusion | flops 786432 | bytes 2622464 | tf_op jit(solution)/shard_map/reduce_sum | solution.py:160
  (31 shorter events, 0.3 us)
Async XLA Ops:
  7.2 162.1 %copy-start = (bf16[1,256,2048]{2,1,0:T(8,128)(2,1)S(1)}, bf16[1,256,2048]{2,1,0:T(8,128)(2,1)}, u32[]{:S(2)}) copy-start(bf16[1,256,2048]{2,1,0:T(8,128)(2,1)} %param.29) | copy-start | bytes 3145732
  7.2 153.4 %all-gather.3.cloned.1.call-start = ((), (), s32[]{:S(2)}) async-start(), calls=%async_computation.5 | async-start | bytes 10485760 | tf_op jit(solution)/shard_map/all_gather | solution.py:140
  103.1 57.5 %copy-start.7 = (bf16[1,2048,256]{2,1,0:T(8,128)(2,1)S(1)}, bf16[1,2048,256]{2,1,0:T(8,128)(2,1)}, u32[]{:S(2)}) copy-start(bf16[1,2048,256]{2,1,0:T(8,128)(2,1)} %param.27) | copy-start | bytes 3145732
  103.1 151.7 %reduce-scatter.2.cloned.1.call-start = ((), (), s32[]{:S(2)}) async-start(), calls=%async_computation.4 | async-start | bytes 10485760 | tf_op jit(solution)/shard_map/reduce_scatter | solution.py:150
  160.6 5.9 %copy-start.6 = (bf16[32,64,2048]{2,1,0:T(8,128)(2,1)S(1)}, bf16[32,64,2048]{2,1,0:T(8,128)(2,1)}, u32[]{:S(2)}) copy-start(bf16[32,64,2048]{2,1,0:T(8,128)(2,1)} %all-gather.3.cloned.1.call-done) | copy-start | bytes 25165828
  160.6 6.0 %copy-start.8 = (bf16[1,2048,256]{2,1,0:T(8,128)(2,1)S(1)}, bf16[1,2048,256]{2,1,0:T(8,128)(2,1)}, u32[]{:S(2)}) copy-start(bf16[1,2048,256]{2,1,0:T(8,128)(2,1)} %param.28) | copy-start | bytes 3145732
  174.8 0.8 copy-start.2
  174.8 33.4 %copy-start.3 = (bf16[256,1,128]{2,0,1:T(8,128)(2,1)S(1)}, bf16[256,1,128]{2,0,1:T(8,128)(2,1)}, u32[]{:S(2)}) copy-start(bf16[256,1,128]{2,0,1:T(8,128)(2,1)} %param.19) | copy-start | bytes 196612
  207.1 32.8 %copy-start.1 = (bf16[256,2,128]{2,1,0:T(2,128)(2,1)S(1)}, bf16[256,2,128]{2,1,0:T(2,128)(2,1)}, u32[]{:S(2)}) copy-start(bf16[256,2,128]{2,1,0:T(2,128)(2,1)} %param.17) | copy-start | bytes 393220
  245.7 1.1 copy-start.4
  245.7 1.6 copy-start.5
  254.8 56.8 %all-to-all-start.2 = ((bf16[1,8,64,2048]{3,2,0,1:T(8,128)(2,1)}), bf16[1,8,64,2048]{3,2,0,1:T(8,128)(2,1)S(1)}, u32[]{:S(2)}, u32[]{:S(2)}) async-start(bf16[1,8,64,2048]{3,2,0,1:T(8,128)(2,1)} %bitcast.127), calls=%async_computation.3 | async-start | bytes 4194304 | tf_op jit(solution)/shard_map/all_to_all | solution.py:158
Sparse Core Ops, SparseCore 0:
  103.2 57.2 all-gather.2
  174.9 71.3 reduce-scatter.1
where the time goes:
time: 331 us; the launch traced here: 330 us
  blocking collectives  125 us (38%)
  waiting for transfers between devices  100 us (30%)
  local copies, waits for them, and re-layouts  49.9 us (15%)
  matrix products  19.2 us (6%)
  between operations  14.4 us (4%)
  other arithmetic  10.6 us (3%)
  starting transfers between devices  9.02 us (3%)
    all_gather x1, waiting for transfers between devices, local(): slot_rows = lax.all_gather(arrived[None], 'tp', axis=0, tiled=True)  57.4 us
    all_to_all x1, blocking collectives, local(): lax.all_to_all(outgoing, 'ep', split_axis=0, concat_axis=0, tiled=True)  55.4 us
    all_to_all x1, waiting for transfers between devices, local(): lax.all_to_all(summed, 'ep', split_axis=1, concat_axis=1, tiled=True)[0]  42.9 us
    scatter x1, local copies, waits for them, and re-layouts, fill_slots(): return (blank_slots.at[block_routes, slot_ids].set(copies), slot_ids)  33.4 us
    all_gather x1, blocking collectives, local(): key_piece = lax.all_gather(keys, 'ep', axis=0, tiled=True)  31.4 us
    all_gather x1, blocking collectives, local(): value_piece = lax.all_gather(values, 'ep', axis=0, tiled=True)  31.4 us
    all_to_all x1, starting transfers between devices, local(): lax.all_to_all(summed, 'ep', split_axis=1, concat_axis=1, tiled=True)[0]  8.94 us
    all_to_all x1, blocking collectives, local(): lax.all_to_all(attn_rows.reshape(positions, q_heads, value_dim), 'tp', sp...  6.99 us
  transfers between devices with their start and end apart: 3, of which 2 were waited for; matrix products, arithmetic and copies ran while one was open for 4% of the time, Pallas kernels for 0%

commit v1 on v0

--- a/solution.py
+++ b/solution.py
@@ -57,8 +57,11 @@
     start_total = jnp.zeros((positions, kv_heads, per_key, 2), jnp.float32)
     start_acc = jnp.zeros((positions, kv_heads, per_key, 2, value_dim), jnp.float32)
     carry = (start_max, start_total, start_acc)
-    key_piece = lax.all_gather(keys, "ep", axis=0, tiled=True)
-    value_piece = lax.all_gather(values, "ep", axis=0, tiled=True)
+    key_piece, value_piece = jnp.split(
+        lax.all_gather(jnp.concatenate([keys, values], axis=1), "ep", axis=0, tiled=True),
+        [keys.shape[1]],
+        axis=1,
+    )
     shard_count = key_piece.shape[0] // positions
     together = 1
     for candidate in (2, 3, 4):

time: 331 us -> 349 us (1.054)
  waiting for transfers between devices: 100 us -> 182 us
  blocking collectives: 125 us -> 62.6 us
    all_gather x2 -> x0, blocking collectives: 62.9 us -> none  [the longest x1 31.4 us: local(): key_piece = lax.all_gather(keys, 'ep', axis=0, tiled=True)]
    reduce_scatter x1, waiting for transfers between devices: 0.01 us -> 54.8 us  [local(): lax.psum_scatter(jnp.dot(flat_terms, w_down[0], preferred_element_type=jn...]
    all_gather x0 -> x1, waiting for transfers between devices: none -> 27.8 us  [local(): lax.all_gather(jnp.concatenate([keys, values], axis=1), 'ep', axis=0, til...]
  transfers between devices with their start and end apart: 3 -> 4, of which waited for: 2 -> 4; matrix products, arithmetic and copies ran while one was open for 4% -> 8% of each run, Pallas kernels for 0% -> 0%
where the time goes in v1:
time: 349 us; the launch traced here: 348 us
  waiting for transfers between devices  182 us (52%)
  blocking collectives  62.6 us (18%)
  local copies, waits for them, and re-layouts  52.1 us (15%)
  matrix products  19.3 us (6%)
  between operations  14 us (4%)
  other arithmetic  11.3 us (3%)
  starting transfers between devices  5.8 us (2%)
    all_gather x1, waiting for transfers between devices, local(): slot_rows = lax.all_gather(arrived[None], 'tp', axis=0, tiled=True)  55.7 us
    all_to_all x1, blocking collectives, local(): lax.all_to_all(outgoing, 'ep', split_axis=0, concat_axis=0, tiled=True)  55.4 us
    reduce_scatter x1, waiting for transfers between devices, local(): lax.psum_scatter(jnp.dot(flat_terms, w_down[0], preferred_element_type=jn...  54.8 us
    all_to_all x1, waiting for transfers between devices, local(): lax.all_to_all(summed, 'ep', split_axis=1, concat_axis=1, tiled=True)[0]  43.2 us
    scatter x1, local copies, waits for them, and re-layouts, fill_slots(): return (blank_slots.at[block_routes, slot_ids].set(copies), slot_ids)  33.4 us
    all_gather x1, waiting for transfers between devices, local(): lax.all_gather(jnp.concatenate([keys, values], axis=1), 'ep', axis=0, til...  27.8 us
    all_to_all x1, blocking collectives, local(): lax.all_to_all(attn_rows.reshape(positions, q_heads, value_dim), 'tp', sp...  7.21 us
  transfers between devices with their start and end apart: 4, of which 4 were waited for; matrix products, arithmetic and copies ran while one was open for 8% of the time, Pallas kernels for 0%

profile of v1, /device:TPU:0, one launch (start us, length us, event | category | flops | bytes accessed | tf_op | source)
XLA Modules:
  0.0 348.1 jit_solution(3404631823822231410)
XLA Ops:
  7.2 0.0 all-gather.6.cloned.1.call-start
  7.2 0.8 constant_dynamic-slice_fusion
  8.0 0.1 copy.83
  8.1 0.1 eq.29
  8.2 0.1 eq.25
  8.4 0.6 reduce-window.6
  9.0 0.2 slice_reduce_fusion
  9.2 0.1 fusion.43
  9.3 0.1 reshape.223
  9.5 0.1 reshape.231
  9.7 1.2 fusion.24
  10.9 1.3 fusion.26
  12.2 0.6 broadcast_in_dim.60
  12.8 1.2 reshape.233
  14.1 0.2 broadcast_in_dim.58
  14.3 33.4 %scatter_fusion = bf16[8,64,2048]{2,1,0:T(8,128)(2,1)S(1)} fusion(bf16[8,64,2048]{2,1,0:T(8,128)(2,1)S(1)} %broadcast_in_dim.58, s32[256]{0:T(256)S(1)} %reshape.231, bf16[256,2048]{1,0:T(8,128)(2,1)} %reshape.233), kind=kCustom, calls=%fused_computation.1 | custom fusion | bytes 3147776 | tf_op jit(solution)/shard_map/scatter | solution.py:27
  47.7 55.4 %all_to_all.25 = bf16[8,64,2048]{2,1,0:T(8,128)(2,1)} all-to-all(bf16[8,64,2048]{2,1,0:T(8,128)(2,1)S(1)} %scatter_fusion), channel_id=1, replica_groups=mesh['ep'=8,'tp'=4] {'ep'}, dimensions={0} | all-to-all | bytes 4194304 | tf_op jit(solution)/shard_map/all_to_all | solution.py:142
  103.1 0.0 all-gather.6.cloned.1.call-update
  103.1 0.0 all-gather.4.cloned.1.call-start
  103.2 0.8 copy-done.2
  103.9 0.0 copy-done.3
  104.0 0.7 pad_maximum_fusion
  104.6 0.0 all-gather.4.cloned.1.call-update
  104.7 0.2 reduce-scatter.2.cloned.1.call-start
  104.9 55.7 %all-gather.6.cloned.1.call-done = bf16[32,64,2048]{2,1,0:T(8,128)(2,1)} async-done(((bf16[8,64,2048]{2,1,0:T(8,128)(2,1)}), bf16[32,64,2048]{2,1,0:T(8,128)(2,1)}) %all-gather.6.cloned.1.call-update) | async-done | bytes 8388624 | tf_op jit(solution)/shard_map/all_gather | solution.py:143
  160.6 5.9 %fusion.29 = f32[2048,256]{1,0:T(8,128)S(1)} fusion(bf16[2048,2048]{1,0:T(8,128)(2,1)} %bitcast.134, bf16[1,2048,256]{2,1,0:T(8,128)(2,1)S(1)} %copy-done.7), kind=kOutput, calls=%fused_computation.40 | convolution fusion | flops 2147483648 | bytes 11534336 | tf_op jit(solution)/shard_map/dot_general | solution.py:145
  166.5 0.1 copy-done.8
  166.6 2.6 fusion.23
  169.2 5.6 %convolution_convert_fusion = bf16[4,8,64,2048]{3,2,1,0:T(8,128)(2,1)} fusion(bf16[4,8,64,256]{3,2,1,0:T(8,128)(2,1)S(1)} %bitcast.130, bf16[1,256,2048]{2,1,0:T(8,128)(2,1)S(1)} %copy-done), kind=kOutput, calls=%fused_computation.28 | convolution fusion | flops 2151677952 | bytes 10485760 | tf_op jit(solution)/shard_map/dot_general | solution.py:154
  174.8 0.0 reduce-scatter.2.cloned.1.call-update
  174.8 0.9 copy-done.1
  175.7 0.1 copy.63
  175.9 27.8 %all-gather.4.cloned.1.call-done = bf16[2048,2,128]{2,0,1:T(8,128)(2,1)} async-done(((bf16[256,2,128]{2,0,1:T(8,128)(2,1)}), bf16[2048,2,128]{2,0,1:T(8,128)(2,1)}) %all-gather.4.cloned.1.call-update) | async-done | bytes 1048592 | tf_op jit(solution)/shard_map/all_gather | solution.py:61
  203.6 1.3 fusion.45
  204.9 0.4 reshape.243
  205.3 0.7 copy.64
  206.1 0.2 copy.66
  206.3 5.9 %while.15 = (s32[]{:T(128)}, f32[256,1,2,2]{0,2,3,1:T(2,128)S(1)}, f32[256,1,2,2]{0,2,3,1:T(2,128)S(1)}, f32[256,1,2,2,128]{0,4,3,2,1:T(8,128)S(1)}, s32[2]{0:T(...) while((s32[]{:T(128)}, f32[256,1,2,2]{0,2,3,1:T(2,128)S(1)}, ...), condition=%wide.region_5.6_spmd.clone, body=%wide.region_0.5_spmd.clone.sunk | while | flops 411570432 | bytes 15155487 | solution.py:107
  206.4 0.6 dynamic_slice.50
  207.6 3.4 conditional.3
  207.6 0.7 iota_add_fusion
  208.3 0.2 broadcast_compare_fusion
  208.5 0.9 fusion.4
  209.4 1.0 fusion.5
  210.4 0.5 fusion.11
  211.0 0.6 dynamic_slice.50
  212.3 0.2 copy.68
  212.5 0.1 copy.67
  212.7 0.7 broadcast_divide_fusion
  213.4 0.4 fusion.33
  213.9 0.4 fusion.37
  214.3 7.2 %all_to_all.26 = bf16[256,2,128]{2,1,0:T(2,128)(2,1)S(1)} all-to-all(bf16[256,2,128]{2,1,0:T(2,128)(2,1)S(1)} %fusion.37), channel_id=1, replica_groups=mesh['ep'=8,'tp'=4] {'tp'}, dimensions={0} | all-to-all | bytes 262144 | tf_op jit(solution)/shard_map/all_to_all | solution.py:117
  221.5 54.8 %reduce-scatter.2.cloned.1.call-done = bf16[1,8,64,2048]{3,2,1,0:T(8,128)(2,1)} async-done(((bf16[4,8,64,2048]{3,2,1,0:T(8,128)(2,1)}), bf16[1,8,64,2048]{3,2,1,0:T(8,128)(2,1)}) %reduce-scatter.2.cloned.1.call-update) | async-done | bytes 2097168 | tf_op jit(solution)/shard_map/reduce_scatter | solution.py:153
  276.4 5.5 %all-to-all-start.2 = ((bf16[1,8,64,2048]{3,2,0,1:T(8,128)(2,1)}), bf16[1,8,64,2048]{3,2,0,1:T(8,128)(2,1)S(1)}, u32[]{:S(2)}, u32[]{:S(2)}) async-start(bf16[1,8,64,2048]{3,2,0,1:T(8,128)(2,1)} %bitcast.127), calls=%async_computation.3 | async-start | bytes 4194304 | tf_op jit(solution)/shard_map/all_to_all | solution.py:161
  281.9 0.1 reshape.225
  282.0 0.7 constant_dynamic-slice_fusion.1
  282.7 0.1 copy.73
  282.8 0.1 copy.72
  283.0 0.1 reshape.221
  283.1 3.7 %convolution_convert_fusion.1 = bf16[64,2048]{1,0:T(8,128)(2,1)} fusion(bf16[64,1024]{1,0:T(8,128)(2,1)S(1)} %reshape.221, bf16[1024,2048]{1,0:T(8,128)(2,1)} %param.22), kind=kOutput, calls=%fused_computation.31 | convolution fusion | flops 268566528 | bytes 4587520 | tf_op jit(solution)/shard_map/dot_general | solution.py:124
  286.8 43.2 %all-to-all-done.2 = bf16[1,8,64,2048]{3,2,0,1:T(8,128)(2,1)S(1)} async-done(((bf16[1,8,64,2048]{3,2,0,1:T(8,128)(2,1)}), bf16[1,8,64,2048]{3,2,0,1:T(8,128)(2,1)S(1)}, u32[]{:S(2)}, u32[]{:S(2)}) %all-to-all-start.2) | async-done | bytes 2097184 | tf_op jit(solution)/shard_map/all_to_all | solution.py:161
  329.9 5.3 %gather_fusion = bf16[256,2048]{1,0:T(8,128)(2,1)} fusion(bf16[8,64,2048]{2,1,0:T(8,128)(2,1)S(1)} %bitcast.126, s32[256]{0:T(256)S(1)} %reshape.225), kind=kCustom, calls=%fused_computation | custom fusion | bytes 2099200 | tf_op jit(solution)/shard_map/gather | solution.py:162
  335.3 2.4 reshape.239
  337.6 3.9 %multiply_reduce_fusion = bf16[128,2048]{1,0:T(8,128)(2,1)} fusion(f32[128,2,2048]{2,1,0:T(2,128)S(1)} %reshape.239, f32[128,2]{1,0:T(8,128)S(1)} %copy.73), kind=kLoop, calls=%fused_computation.32 | loop fusion | flops 786432 | bytes 2622464 | tf_op jit(solution)/shard_map/reduce_sum | solution.py:163
  (34 shorter events, 0.3 us)
Async XLA Ops:
  7.2 162.1 %copy-start = (bf16[1,256,2048]{2,1,0:T(8,128)(2,1)S(1)}, bf16[1,256,2048]{2,1,0:T(8,128)(2,1)}, u32[]{:S(2)}) copy-start(bf16[1,256,2048]{2,1,0:T(8,128)(2,1)} %param.29) | copy-start | bytes 3145732
  7.2 153.4 %all-gather.6.cloned.1.call-start = ((), (), s32[]{:S(2)}) async-start(), calls=%async_computation.6 | async-start | bytes 10485760 | tf_op jit(solution)/shard_map/all_gather | solution.py:143
  103.1 0.8 copy-start.2
  103.1 0.9 copy-start.3
  103.1 57.5 %copy-start.7 = (bf16[1,2048,256]{2,1,0:T(8,128)(2,1)S(1)}, bf16[1,2048,256]{2,1,0:T(8,128)(2,1)}, u32[]{:S(2)}) copy-start(bf16[1,2048,256]{2,1,0:T(8,128)(2,1)} %param.27) | copy-start | bytes 3145732
  103.1 100.5 %all-gather.4.cloned.1.call-start = ((), (), s32[]{:S(2)}) async-start(), calls=%async_computation.4 | async-start | bytes 1179648 | tf_op jit(solution)/shard_map/all_gather | solution.py:61
  104.7 171.7 %reduce-scatter.2.cloned.1.call-start = ((), (), s32[]{:S(2)}) async-start(), calls=%async_computation.5 | async-start | bytes 10485760 | tf_op jit(solution)/shard_map/reduce_scatter | solution.py:153
  160.6 5.9 %copy-start.6 = (bf16[32,64,2048]{2,1,0:T(8,128)(2,1)S(1)}, bf16[32,64,2048]{2,1,0:T(8,128)(2,1)}, u32[]{:S(2)}) copy-start(bf16[32,64,2048]{2,1,0:T(8,128)(2,1)} %all-gather.6.cloned.1.call-done) | copy-start | bytes 25165828
  160.6 6.0 %copy-start.8 = (bf16[1,2048,256]{2,1,0:T(8,128)(2,1)S(1)}, bf16[1,2048,256]{2,1,0:T(8,128)(2,1)}, u32[]{:S(2)}) copy-start(bf16[1,2048,256]{2,1,0:T(8,128)(2,1)} %param.28) | copy-start | bytes 3145732
  174.8 0.9 copy-start.1
  212.3 1.1 copy-start.4
  212.3 1.6 copy-start.5
  276.4 53.6 %all-to-all-start.2 = ((bf16[1,8,64,2048]{3,2,0,1:T(8,128)(2,1)}), bf16[1,8,64,2048]{3,2,0,1:T(8,128)(2,1)S(1)}, u32[]{:S(2)}, u32[]{:S(2)}) async-start(bf16[1,8,64,2048]{3,2,0,1:T(8,128)(2,1)} %bitcast.127), calls=%async_computation.3 | async-start | bytes 4194304 | tf_op jit(solution)/shard_map/all_to_all | solution.py:161
Sparse Core Ops, SparseCore 0:
  103.2 57.2 all-gather.5
  163.3 40.2 all-gather.3
  206.2 70.1 reduce-scatter.1
